TPU v7x, 256 devices: a whole 4x4x8 slice. The times are simulated.
256 devices in a mesh: ep: 16 (over y, x), tp: 16 (over z, core).
Axes of the slice: x: 4, y: 4, z: 8, core: 2. Of those that a mesh axis runs over, the one named last changes fastest.
Arguments:
- mix_tokens: bfloat16 [4096, 4096], P('ep'), may hold values from -6 to 6
- mix_gain: float32 [4096], replicated, may hold values from 0.1 to 1.9
- value_weight: bfloat16 [4096, 2048], P(None, 'tp'), may hold values from -0.09375 to 0.09375
- inner_weight: bfloat16 [4096, 2048], P(None, 'tp'), may hold values from -0.09375 to 0.09375
- outer_weight: bfloat16 [4096, 2048], P(None, 'tp'), may hold values from -0.09375 to 0.09375
- conv_taps: float32 [3, 2048], P(None, 'tp'), may hold values from -3 to 3
- mix_weight: bfloat16 [2048, 4096], P('tp'), may hold values from -0.125 to 0.125
- moe_tokens: bfloat16 [4096, 4096], P('ep'), may hold values from -6 to 6
- moe_gain: float32 [4096], replicated, may hold values from 0.1 to 1.9
- router_group: bfloat16 [4096, 4], replicated, may hold values from -0.09375 to 0.09375
- router_expert: bfloat16 [4096, 16], replicated, may hold values from -0.09375 to 0.09375
- expert_routes: int32 [4096, 2], P('ep'), may hold values from 0 to 15, as said below
- gate_weight: bfloat16 [16, 4096, 2048], P('ep', None, 'tp'), may hold values from -0.09375 to 0.09375
- up_weight: bfloat16 [16, 4096, 2048], P('ep', None, 'tp'), may hold values from -0.09375 to 0.09375
- down_weight: bfloat16 [16, 2048, 4096], P('ep', 'tp'), may hold values from -0.5 to 0.5
Outputs:
- mixer_out: bfloat16 [4096, 4096], P(('ep', 'tp'))
- expert_out: bfloat16 [4096, 4096], P(('ep', 'tp'))
Inputs may be any that keep to these rules, and one draw needn't show every extreme that they name: `expert_routes`: the two experts of a row are different and lie in one group of 4 consecutive expert numbers. In each aligned block of 16 rows no expert is named more than 4 times, and in every draw some experts are named exactly 4 times in every block.
All inputs are finite; a program needn't handle non-finite values.
Results may differ from a plain program's by a relative error of at most 0.0076.
Values may be sent and summed in bfloat16 or wider, within the bound.
No kernel may reach another device: no remote copies, remote signals or barrier semaphores. Data moves between devices by JAX's collectives and lax.ppermute only.
A program may use at most 128 MiB of HBM per device.

v0:
```python
import jax
import jax.numpy as jnp
from jax import lax
from jax.sharding import PartitionSpec as P

TAPS = 3
EXPERTS = 16
GROUPS = 4
TOPK = 2
MOE_SHARE = 16
EPG = 4
CAP = 4


def from_behind(value, axis, steps):
    count = lax.axis_size(axis)
    initial, last = (max(0, -steps), min(count, count - steps))
    return lax.ppermute(value, axis, [(source, source + steps) for source in range(initial, last)])


def rms_rows(inputs, gain_vec):
    values = inputs.astype(jnp.float32)
    inverse = lax.rsqrt(jnp.mean(values * values, axis=-1, keepdims=True) + 1e-06)
    return (values * inverse * gain_vec).astype(jnp.bfloat16)


def route_weights(normed, routes, router_group, router_expert):
    group_logit = jnp.dot(normed, router_group, preferred_element_type=jnp.float32)
    expert_logit = jnp.dot(normed, router_expert, preferred_element_type=jnp.float32)
    group_exp = jnp.exp(group_logit)
    group_id = routes[:, 0] // EPG
    group_pick = (group_id[:, None] == jnp.arange(GROUPS, dtype=jnp.int32)[None, :]).astype(
        jnp.float32
    )
    group_gate = jnp.sum(group_exp * group_pick, axis=1) / jnp.sum(group_exp, axis=1)
    expert_pick = (
        routes[:, :, None] == jnp.arange(EXPERTS, dtype=jnp.int32)[None, None, :]
    ).astype(jnp.float32)
    chosen = jnp.exp(jnp.sum(expert_logit[:, None, :] * expert_pick, axis=2))
    return group_gate[:, None] * chosen / jnp.sum(chosen, axis=1, keepdims=True)


def block_ranks(routes):
    blocks = routes.shape[0]
    entries = routes.reshape(blocks, MOE_SHARE * TOPK)
    one_hot = (entries[:, :, None] == jnp.arange(EXPERTS, dtype=jnp.int32)[None, None, :]).astype(
        jnp.int32
    )
    before = jnp.cumsum(one_hot, axis=1) - one_hot
    return jnp.sum(before * one_hot, axis=2).reshape(routes.shape)


def dispatch_rows(normed, routes):
    slot_ids = routes * CAP + block_ranks(routes)
    targets = jnp.arange(EXPERTS * CAP, dtype=jnp.int32)
    select = (slot_ids[:, None, :, :] == targets[None, :, None, None]).astype(jnp.int32)
    select = jnp.sum(select, axis=3).astype(jnp.bfloat16)
    placed = jnp.einsum("bcs,bsd->bcd", select, normed, preferred_element_type=jnp.float32)
    return placed.astype(jnp.bfloat16).reshape(normed.shape[0], EXPERTS, CAP, normed.shape[2])


def expert_hidden(arrived, gate_weight, up_weight):
    gate_proj = jnp.einsum(
        "besd,edf->besf", arrived, gate_weight, preferred_element_type=jnp.float32
    )
    up_proj = jnp.einsum("besd,edf->besf", arrived, up_weight, preferred_element_type=jnp.float32)
    return (jax.nn.silu(gate_proj) * up_proj).astype(jnp.bfloat16)


def mixer_half(
    mix_tokens, mix_gain, value_weight, inner_weight, outer_weight, conv_taps, mix_weight
):
    normed = rms_rows(mix_tokens, mix_gain)
    value_proj = jnp.dot(normed, value_weight, preferred_element_type=jnp.float32)
    inner_proj = jnp.dot(normed, inner_weight, preferred_element_type=jnp.float32)
    outer_proj = jnp.dot(normed, outer_weight, preferred_element_type=jnp.float32)
    gated_in = (inner_proj * value_proj).astype(jnp.bfloat16)
    earlier = from_behind(gated_in[gated_in.shape[0] - (TAPS - 1) :], "ep", 1)
    padded = jnp.concatenate([earlier, gated_in], axis=0).astype(jnp.float32)
    seq_rows = gated_in.shape[0]
    mixed_conv = conv_taps[0] * padded[0:seq_rows]
    for tap_index in range(1, TAPS):
        mixed_conv = mixed_conv + conv_taps[tap_index] * padded[tap_index : tap_index + seq_rows]
    conv_out = (outer_proj * mixed_conv).astype(jnp.bfloat16)
    summed = lax.psum_scatter(
        jnp.dot(conv_out, mix_weight, preferred_element_type=jnp.float32),
        "tp",
        scatter_dimension=0,
        tiled=True,
    )
    return summed.astype(jnp.bfloat16)


def local(
    mix_tokens,
    mix_gain,
    value_weight,
    inner_weight,
    outer_weight,
    conv_taps,
    mix_weight,
    moe_tokens,
    moe_gain,
    router_group,
    router_expert,
    expert_routes,
    gate_weight,
    up_weight,
    down_weight,
):
    mixer_out = mixer_half(
        mix_tokens, mix_gain, value_weight, inner_weight, outer_weight, conv_taps, mix_weight
    )
    tp_index = lax.axis_index("tp")
    model_width = moe_tokens.shape[1]
    own_routes = lax.dynamic_slice_in_dim(expert_routes, tp_index * MOE_SHARE, MOE_SHARE, 0)
    own_tokens = lax.dynamic_slice_in_dim(moe_tokens, tp_index * MOE_SHARE, MOE_SHARE, 0)
    own_normed = rms_rows(own_tokens, moe_gain)
    placed = dispatch_rows(own_normed[None], own_routes[None])[0]
    arrived = lax.all_to_all(placed, "ep", split_axis=0, concat_axis=1, tiled=True)
    hidden = expert_hidden(
        lax.all_gather(arrived[None], "tp", axis=0, tiled=True), gate_weight, up_weight
    )
    local_experts = hidden.shape[1]
    slot_count = hidden.shape[2]
    per_block = local_experts * slot_count
    partial_value = jnp.einsum(
        "besf,efd->besd", hidden, down_weight, preferred_element_type=jnp.float32
    )
    summed = lax.psum_scatter(
        partial_value.reshape(per_block * lax.axis_size("tp"), model_width),
        "tp",
        scatter_dimension=0,
        tiled=True,
    )
    results = summed.astype(jnp.bfloat16).reshape(
        local_experts, slot_count // CAP, CAP, model_width
    )
    returned = lax.all_to_all(results, "ep", split_axis=1, concat_axis=0, tiled=True).reshape(
        EXPERTS * CAP, model_width
    )
    weights = route_weights(own_normed, own_routes, router_group, router_expert)
    own_slots = own_routes * CAP + block_ranks(own_routes[None])[0]
    picked = jnp.take(returned, own_slots, axis=0).astype(jnp.float32)
    expert_out = jnp.sum(weights[:, :, None] * picked, axis=1).astype(jnp.bfloat16)
    return (mixer_out, expert_out)


def solution(mesh):
    return jax.shard_map(
        local,
        mesh=mesh,
        in_specs=(
            P("ep", None),
            P(),
            P(None, "tp"),
            P(None, "tp"),
            P(None, "tp"),
            P(None, "tp"),
            P("tp", None),
            P("ep", None),
            P(),
            P(),
            P(),
            P("ep", None),
            P("ep", None, "tp"),
            P("ep", None, "tp"),
            P("ep", "tp", None),
        ),
        out_specs=(P(("ep", "tp"), None), P(("ep", "tp"), None)),
        check_vma=False,
    )
```

profile of v0, /device:TPU:2, one launch (start us, length us, event | category | flops | bytes accessed | tf_op | source)
XLA Modules:
  0.0 281.7 jit_solution(8360812834643250856)
XLA Ops:
  7.2 0.0 copy-start
  7.2 0.0 all-gather.2.cloned.1.call-start
  7.2 0.8 constant_dynamic-slice_fusion
  8.1 0.1 copy.25
  8.1 0.1 eq.90
  8.2 0.1 fusion.48
  8.3 0.1 reduce_window_sum.12
  8.4 0.2 select_reduce_fusion
  8.6 0.1 squeeze_reshape.6
  8.6 0.1 copy.26
  8.7 0.8 compare_and_fusion
  9.5 0.1 convert_reduce_fusion
  9.6 1.0 fusion.37
  10.6 1.3 convolution_convert_fusion
  11.9 0.2 squeeze_reshape.7
  12.1 17.4 %all_to_all.8 = bf16[16,4,4096]{2,1,0:T(4,128)(2,1)S(1)} all-to-all(bf16[16,4,4096]{2,1,0:T(4,128)(2,1)S(1)} %squeeze_reshape.7), channel_id=1, replica_groups=mesh['ep'=16,'tp'=16] {'ep'}, dimensions={0} | all-to-all | bytes 1048576 | tf_op jit(solution)/shard_map/all_to_all | solution.py:120
  29.5 0.9 broadcast_in_dim.12
  30.5 0.0 all-gather.2.cloned.1.call-update
  30.5 0.0 copy-start.2
  30.5 0.0 reduce-scatter.5.cloned.1.call-start
  30.5 55.9 %all-gather.2.cloned.1.call-done = bf16[16,1,64,4096]{3,2,1,0:T(8,128)(2,1)} async-done(((bf16[1,1,64,4096]{3,2,1,0:T(8,128)(2,1)}), bf16[16,1,64,4096]{3,2,1,0:T(8,128)(2,1)}) %all-gather.2.cloned.1.call-update) | async-done | bytes 8388624 | tf_op jit(solution)/shard_map/all_gather | solution.py:122
  86.5 5.9 %fusion.7 = f32[16,1,64,128]{3,2,0,1:T(8,128)S(1)} fusion(bf16[16,1,64,4096]{3,2,1,0:T(8,128)(2,1)} %all-gather.2.cloned.1.call-done, bf16[1,4096,128]{2,1,0:T(8,128)(2,1)} %param.27), kind=kOutput, calls=%fused_computation.11 | convolution fusion | flops 1073741824 | bytes 9961472 | tf_op jit(solution)/shard_map/besd,edf->besf/dot_general | solution.py:63
  92.4 0.0 copy-done
  92.4 0.0 copy-done.2
  92.4 14.4 %fusion.23 = f32[16,64,4096]{2,1,0:T(8,128)} fusion(bf16[16,1,64,4096]{3,2,1,0:T(8,128)(2,1)} %all-gather.2.cloned.1.call-done, bf16[1,128,4096]{2,1,0:T(8,128)(2,1)S(1)} %copy-done, bf16[1,4096,128]{2,1,0:T(8,128)(2,1)S(1)} %copy-done.2, f32[16,1,64,128]{3,2,0,1:T(8,128)S(1)} %fusion.7), kind=kOutput, calls=%fused_computation.16 | convolution fusion | flops 2148270080 | bytes 27787264 | tf_op jit(solution)/shard_map/besf,efd->besd/dot_general | solution.py:127
  106.8 0.0 copy-start.1
  106.8 0.0 copy-start.3
  106.8 0.0 reduce-scatter.5.cloned.1.call-update
  106.8 0.0 reduce-scatter.3.cloned.1.call-start
  106.9 1.5 copy-done.1
  108.4 0.0 copy-start.6
  108.4 0.5 fusion.4
  108.9 0.0 copy-done.3
  108.9 0.0 copy-start.5
  108.9 2.1 fusion.57
  111.0 0.0 copy-done.6
  111.0 0.9 fusion.26
  111.9 3.4 %collective-permute-start = (bf16[2,128]{1,0:T(2,128)(2,1)S(1)}, bf16[2,128]{1,0:T(2,128)(2,1)S(1)}, u32[]{:S(2)}, u32[]{:S(2)}) collective-permute-start(bf16[2,128]{1,0:T(2,128)(2,1)S(1)} %slice.34), channel_id=1, source_target_pairs={{0,16},{16,32},{32,48},{48,64},{64,80},{80,96},{96,112},{112,128},... | collective-permute-start | bytes 1544 | tf_op jit(solution)/shard_map/ppermute | solution.py:18
  115.3 0.0 copy-done.5
  115.3 2.1 collective-permute-done
  117.4 5.0 %fusion.27 = f32[256,4096]{1,0:T(8,128)} fusion(bf16[128,4096]{1,0:T(8,128)(2,1)} %param.21, bf16[4096,128]{1,0:T(8,128)(2,1)} %param.19, f32[258,128]{1,0:T(8,128)S(1)} %maximum_convert_fusion, f32[128]{0:T(128)S(1)} %get-tuple-element.7, f32[128]{0:T(128)S(1)} %get-tuple-element.8, f32[128]{0:T(128)S(1)} %get-tuple-element.6, ...), kind=kOutput, calls=%fused_computation.21 | convolution fusion | flops 541294592 | bytes 8800768 | tf_op jit(solution)/shard_map/dot_general | solution.py:86
  122.4 0.0 copy-start.4
  122.4 0.0 reduce-scatter.3.cloned.1.call-update
  122.4 0.7 copy-done.4
  123.1 0.1 copy-done.8
  123.1 1.2 fusion.61
  124.3 0.0 copy-done.7
  124.3 1.1 fusion.53
  125.5 80.6 %reduce-scatter.5.cloned.1.call-done = f32[64,4096]{1,0:T(8,128)} async-done(((f32[1024,4096]{1,0:T(8,128)}), f32[64,4096]{1,0:T(8,128)}) %reduce-scatter.5.cloned.1.call-update) | async-done | bytes 1048592 | tf_op jit(solution)/shard_map/reduce_scatter | solution.py:130
  206.1 1.3 convert_element_type.92
  207.4 1.0 reshape.229
  208.4 7.3 %all-to-all-start.1 = ((bf16[1,16,4,4096]{3,2,0,1:T(4,128)(2,1)}), bf16[1,16,4,4096]{3,2,0,1:T(4,128)(2,1)S(1)}, u32[]{:S(2)}, u32[]{:S(2)}) async-start(bf16[1,16,4,4096]{3,2,0,1:T(4,128)(2,1)} %reshape.229), calls=%async_computation.3 | async-start | bytes 1048576 | tf_op jit(solution)/shard_map/all_to_all | solution.py:139
  215.6 0.2 select_reduce_fusion.1
  215.8 0.1 copy.28
  215.9 0.1 reshape.233
  216.0 0.1 copy.24
  216.1 0.1 copy.27
  216.2 54.8 %reduce-scatter.3.cloned.1.call-done = f32[16,4096]{1,0:T(8,128)} async-done(((f32[256,4096]{1,0:T(8,128)}), f32[16,4096]{1,0:T(8,128)}) %reduce-scatter.3.cloned.1.call-update) | async-done | bytes 262160 | tf_op jit(solution)/shard_map/reduce_scatter | solution.py:85
  271.0 1.6 convert_element_type.84
  272.7 0.0 all-to-all-done.1
  272.7 0.1 reshape.230
  272.8 0.7 gather_fusion
  273.5 0.2 reshape.232
  273.7 1.5 multiply_reduce_fusion
  (13 shorter events, 0.1 us)
Async XLA Ops:
  7.2 85.2 %copy-start = (bf16[1,128,4096]{2,1,0:T(8,128)(2,1)S(1)}, bf16[1,128,4096]{2,1,0:T(8,128)(2,1)}, u32[]{:S(2)}) copy-start(bf16[1,128,4096]{2,1,0:T(8,128)(2,1)} %param.29) | copy-start | bytes 3145732
  7.2 79.3 %all-gather.2.cloned.1.call-start = ((), (), s32[]{:S(2)}) async-start(), calls=%async_computation.5 | async-start | bytes 8912896 | tf_op jit(solution)/shard_map/all_gather | solution.py:122
  30.5 61.9 %copy-start.2 = (bf16[1,4096,128]{2,1,0:T(8,128)(2,1)S(1)}, bf16[1,4096,128]{2,1,0:T(8,128)(2,1)}, u32[]{:S(2)}) copy-start(bf16[1,4096,128]{2,1,0:T(8,128)(2,1)} %param.28) | copy-start | bytes 3145732
  30.5 175.6 %reduce-scatter.5.cloned.1.call-start = ((), (), s32[]{:S(2)}) async-start(), calls=%async_computation.6 | async-start | bytes 17825792 | tf_op jit(solution)/shard_map/reduce_scatter | solution.py:130
  106.8 1.6 copy-start.1
  106.8 2.1 copy-start.3
  106.8 164.2 %reduce-scatter.3.cloned.1.call-start = ((), (), s32[]{:S(2)}) async-start(), calls=%async_computation.4 | async-start | bytes 4456448 | tf_op jit(solution)/shard_map/reduce_scatter | solution.py:85
  108.4 2.6 copy-start.6
  108.9 6.4 %copy-start.5 = (f32[3,128]{1,0:T(4,128)S(1)}, f32[3,128]{1,0:T(4,128)}, u32[]{:S(2)}) copy-start(f32[3,128]{1,0:T(4,128)} %param.20) | copy-start | bytes 4612
  111.9 5.5 %collective-permute-start = (bf16[2,128]{1,0:T(2,128)(2,1)S(1)}, bf16[2,128]{1,0:T(2,128)(2,1)S(1)}, u32[]{:S(2)}, u32[]{:S(2)}) collective-permute-start(bf16[2,128]{1,0:T(2,128)(2,1)S(1)} %slice.34), channel_id=1, source_target_pairs={{0,16},{16,32},{32,48},{48,64},{64,80},{80,96},{96,112},{112,128},... | collective-permute-start | bytes 1544 | tf_op jit(solution)/shard_map/ppermute | solution.py:18
  122.4 0.7 copy-start.4
  122.4 0.8 copy-start.8
  122.4 1.9 copy-start.7
  208.4 64.3 %all-to-all-start.1 = ((bf16[1,16,4,4096]{3,2,0,1:T(4,128)(2,1)}), bf16[1,16,4,4096]{3,2,0,1:T(4,128)(2,1)S(1)}, u32[]{:S(2)}, u32[]{:S(2)}) async-start(bf16[1,16,4,4096]{3,2,0,1:T(4,128)(2,1)} %reshape.229), calls=%async_computation.3 | async-start | bytes 1048576 | tf_op jit(solution)/shard_map/all_to_all | solution.py:139
Sparse Core Ops, SparseCore 0:
  30.6 55.8 all-gather.1
  107.0 99.0 reduce-scatter.4
  208.6 62.3 reduce-scatter.2
where the time goes:
time: 282 us
  waiting for transfers between devices  193 us (68%)
  matrix products  31.8 us (11%)
  blocking collectives  17.4 us (6%)
  between operations  14 us (5%)
  starting transfers between devices  10.8 us (4%)
  other arithmetic  7.33 us (3%)
  local copies, waits for them, and re-layouts  6.92 us (2%)
    reduce_scatter x1, waiting for transfers between devices, local(): lax.psum_scatter(partial_value.reshape(per_block * lax.axis_size('tp'), m...  80.6 us
    all_gather x1, waiting for transfers between devices, local(): lax.all_gather(arrived[None], 'tp', axis=0, tiled=True)  55.9 us
    reduce_scatter x1, waiting for transfers between devices, mixer_half(): lax.psum_scatter(jnp.dot(conv_out, mix_weight, preferred_element_type=jnp...  54.8 us
    all_to_all x1, blocking collectives, local(): lax.all_to_all(placed, 'ep', split_axis=0, concat_axis=1, tiled=True)  17.4 us
    dot_general x1, matrix products, local(): jnp.einsum('besf,efd->besd', hidden, down_weight, preferred_element_type=...  14.4 us
    all_to_all x1, starting transfers between devices, local(): lax.all_to_all(results, 'ep', split_axis=1, concat_axis=0, tiled=True)  7.27 us
    dot_general x1, matrix products, expert_hidden(): jnp.einsum('besd,edf->besf', arrived, gate_weight, preferred_element_type...  5.93 us
  transfers between devices with their start and end apart: 5, of which 4 were waited for; matrix products, arithmetic and copies ran while one was open for 5% of the time, Pallas kernels for 0%

commit v1 on v0

--- a/solution.py
+++ b/solution.py
@@ -10,6 +10,24 @@
 MOE_SHARE = 16
 EPG = 4
 CAP = 4
+
+
+def proceed_threads_over_axis(x0, dim_i):
+    x0 = jnp.moveaxis(x0, 0, dim_i)
+    s_next = x0.shape
+    return x0.reshape(*s_next[:dim_i], s_next[dim_i] * s_next[dim_i + 1], *s_next[dim_i + 2 :])
+
+
+def _state_vector(here_x, axis_tag):
+    ready = lax.axis_size(axis_tag)
+    clean, block_out = (ready, lax.axis_index(axis_tag))
+    formed, z_new = (here_x[None], 1)
+    while z_new < clean:
+        upper = lax.ppermute(formed, axis_tag, [(pp, pp ^ z_new) for pp in range(clean)])
+        odd = block_out & z_new == 0
+        formed = jnp.concatenate([jnp.where(odd, formed, upper), jnp.where(odd, upper, formed)])
+        z_new *= 2
+    return formed
 
 
 def from_behind(value, axis, steps):
@@ -118,9 +136,12 @@
     own_normed = rms_rows(own_tokens, moe_gain)
     placed = dispatch_rows(own_normed[None], own_routes[None])[0]
     arrived = lax.all_to_all(placed, "ep", split_axis=0, concat_axis=1, tiled=True)
-    hidden = expert_hidden(
-        lax.all_gather(arrived[None], "tp", axis=0, tiled=True), gate_weight, up_weight
-    )
+
+    def face_test(mine, mat, in_dim=0):
+        top = _state_vector(mine, mat)
+        return proceed_threads_over_axis(top, in_dim)
+
+    hidden = expert_hidden(face_test(arrived[None], "tp"), gate_weight, up_weight)
     local_experts = hidden.shape[1]
     slot_count = hidden.shape[2]
     per_block = local_experts * slot_count

time: 282 us -> 542 us (1.92)
  waiting for transfers between devices: 193 us -> 433 us
  starting transfers between devices: 10.8 us -> 21.2 us
  other arithmetic: 7.33 us -> 16.9 us
    ppermute x0 -> x4, waiting for transfers between devices: none -> 297 us  [_state_vector(): lax.ppermute(formed, axis_tag, [(pp, pp ^ z_new) for pp in range(clean)])]
    all_gather x1 -> x0, waiting for transfers between devices: 55.9 us -> none  [local(): lax.all_gather(arrived[None], 'tp', axis=0, tiled=True)]
    ppermute x0 -> x4, starting transfers between devices: none -> 11.5 us  [_state_vector(): lax.ppermute(formed, axis_tag, [(pp, pp ^ z_new) for pp in range(clean)])]
    select_n x0 -> x4, other arithmetic: none -> 5.75 us  [_state_vector(): jnp.where(odd, formed, upper)]
  transfers between devices with their start and end apart: 5 -> 8, of which waited for: 4 -> 7; matrix products, arithmetic and copies ran while one was open for 5% -> 3% of each run, Pallas kernels for 0% -> 0%
where the time goes in v1:
time: 542 us
  waiting for transfers between devices  433 us (80%)
  matrix products  28.2 us (5%)
  starting transfers between devices  21.2 us (4%)
  blocking collectives  17.4 us (3%)
  other arithmetic  16.9 us (3%)
  between operations  14.4 us (3%)
  local copies, waits for them, and re-layouts  10.5 us (2%)
    ppermute x4, waiting for transfers between devices, _state_vector(): lax.ppermute(formed, axis_tag, [(pp, pp ^ z_new) for pp in range(clean)])  297 us
    reduce_scatter x1, waiting for transfers between devices, local(): lax.psum_scatter(partial_value.reshape(per_block * lax.axis_size('tp'), m...  78.3 us
    reduce_scatter x1, waiting for transfers between devices, mixer_half(): lax.psum_scatter(jnp.dot(conv_out, mix_weight, preferred_element_type=jnp...  54.6 us
    all_to_all x1, blocking collectives, local(): lax.all_to_all(placed, 'ep', split_axis=0, concat_axis=1, tiled=True)  17.4 us
    dot_general x1, matrix products, local(): jnp.einsum('besf,efd->besd', hidden, down_weight, preferred_element_type=...  14.4 us
    ppermute x4, starting transfers between devices, _state_vector(): lax.ppermute(formed, axis_tag, [(pp, pp ^ z_new) for pp in range(clean)])  11.5 us
  transfers between devices with their start and end apart: 8, of which 7 were waited for; matrix products, arithmetic and copies ran while one was open for 3% of the time, Pallas kernels for 0%

profile of v1, /device:TPU:2, one launch (start us, length us, event | category | flops | bytes accessed | tf_op | source)
XLA Modules:
  0.0 541.7 jit_solution(15432439459084749076)
XLA Ops:
  7.2 0.8 constant_dynamic-slice_fusion
  8.1 0.1 copy.25
  8.1 0.1 eq.102
  8.2 0.1 fusion.29
  8.3 0.1 reduce_window_sum.12
  8.4 0.2 select_reduce_fusion
  8.6 0.1 squeeze_reshape.6
  8.6 0.1 copy.26
  8.7 0.8 compare_and_fusion
  9.5 0.1 convert_reduce_fusion
  9.6 1.0 fusion.14
  10.6 1.3 convolution_convert_fusion
  11.9 0.2 squeeze_reshape.7
  12.1 17.4 %all_to_all.8 = bf16[16,4,4096]{2,1,0:T(4,128)(2,1)S(1)} all-to-all(bf16[16,4,4096]{2,1,0:T(4,128)(2,1)S(1)} %squeeze_reshape.7), channel_id=1, replica_groups=mesh['ep'=16,'tp'=16] {'ep'}, dimensions={0} | all-to-all | bytes 1048576 | tf_op jit(solution)/shard_map/all_to_all | solution.py:138
  29.6 0.1 broadcast_in_dim_broadcast_in_dim.3
  29.7 0.1 collective-permute-start.1
  29.8 1.9 collective-permute-done.1
  31.7 0.1 broadcast_select_fusion.7
  31.8 1.1 pad_maximum_fusion.2
  32.8 1.9 collective-permute-start.2
  34.7 23.7 %collective-permute-done.2 = bf16[2,1,1,64,4096]{4,3,0,2,1:T(8,128)(2,1)S(1)} collective-permute-done((bf16[2,1,1,64,4096]{4,3,0,2,1:T(8,128)(2,1)}, bf16[2,1,1,64,4096]{4,3,0,2,1:T(8,128)(2,1)S(1)}, u32[]{:S(2)}, u32[]{:S(2)}) %collective-permute-start.2) | collective-permute-done | bytes 1048608 | tf_op jit(solution)/shard_map/ppermute | solution.py:26
  58.4 0.1 broadcast_select_fusion.5
  58.6 1.0 copy-done.5
  59.5 0.2 pad_maximum_fusion.1
  59.7 0.1 copy-done.6
  59.9 3.3 collective-permute-start.3
  63.1 90.3 %collective-permute-done.3 = bf16[4,1,1,64,4096]{4,3,0,2,1:T(8,128)(2,1)} collective-permute-done((bf16[4,1,1,64,4096]{4,3,0,2,1:T(8,128)(2,1)S(1)}, bf16[4,1,1,64,4096]{4,3,0,2,1:T(8,128)(2,1)}, u32[]{:S(2)}, u32[]{:S(2)}) %collective-permute-start.3) | collective-permute-done | bytes 2097184 | tf_op jit(solution)/shard_map/ppermute | solution.py:26
  153.4 2.4 broadcast_select_fusion.3
  155.9 2.6 pad_maximum_fusion
  158.4 0.1 copy-done.2
  158.5 6.2 %collective-permute-start.4 = (bf16[8,1,1,64,4096]{4,3,0,2,1:T(8,128)(2,1)}, bf16[8,1,1,64,4096]{4,3,0,2,1:T(8,128)(2,1)}, u32[]{:S(2)}, u32[]{:S(2)}) collective-permute-start(bf16[8,1,1,64,4096]{4,3,0,2,1:T(8,128)(2,1)} %pad_maximum_fusion), channel_id=1, source_target_pairs={{0,8},{1,9},{2,10},{3,11},{4,12},{5,13},{6,14},{7,15},{8,0},{9,1},... | collective-permute-start | bytes 12582920 | tf_op jit(solution)/shard_map/ppermute | solution.py:26
  164.7 181.3 %collective-permute-done.4 = bf16[8,1,1,64,4096]{4,3,0,2,1:T(8,128)(2,1)} collective-permute-done((bf16[8,1,1,64,4096]{4,3,0,2,1:T(8,128)(2,1)}, bf16[8,1,1,64,4096]{4,3,0,2,1:T(8,128)(2,1)}, u32[]{:S(2)}, u32[]{:S(2)}) %collective-permute-start.4) | collective-permute-done | bytes 4194336 | tf_op jit(solution)/shard_map/ppermute | solution.py:26
  346.0 3.1 broadcast_select_fusion.1
  349.1 1.9 copy-done.3
  351.1 1.2 copy-done.4
  352.3 2.5 fusion.5
  354.9 14.4 %fusion.10 = f32[16,64,4096]{2,1,0:T(8,128)} fusion(bf16[1,128,4096]{2,1,0:T(8,128)(2,1)S(1)} %copy-done, f32[16,1,64,128]{3,2,0,1:T(8,128)S(1)} %fusion.5, bf16[8,1,1,64,4096]{4,3,0,2,1:T(8,128)(2,1)} %copy-done.4, bf16[8,1,1,64,4096]{4,3,0,2,1:T(8,128)(2,1)} %copy-done.3, bf16[1,4096,128]{2,1,0:T(8,128)(2,1)S(1)} %copy-done.9), kind=kOutput, calls=%fused_computation.25 | convolution fusion | flops 2152464384 | bytes 27787264 | tf_op jit(solution)/shard_map/besf,efd->besd/dot_general | solution.py:148
  369.3 0.0 reduce-scatter.3.cloned.1.call-start
  369.4 1.5 copy-done.7
  370.9 0.5 fusion.2
  371.4 2.1 fusion.41
  373.6 0.9 fusion.8
  374.4 2.3 collective-permute-start
  376.8 3.1 collective-permute-done
  379.9 4.6 fusion.9
  384.6 0.7 copy-done.11
  385.3 0.1 copy-done.16
  385.3 1.2 fusion.45
  386.5 1.2 fusion.37
  387.7 78.3 %reduce-scatter.5.cloned.1.call-done = f32[64,4096]{1,0:T(8,128)} async-done(((f32[1024,4096]{1,0:T(8,128)}), f32[64,4096]{1,0:T(8,128)}) %reduce-scatter.5.cloned.1.call-update) | async-done | bytes 1048592 | tf_op jit(solution)/shard_map/reduce_scatter | solution.py:151
  466.0 1.3 convert_element_type.92
  467.3 1.0 reshape.232
  468.3 7.3 %all-to-all-start.1 = ((bf16[1,16,4,4096]{3,2,0,1:T(4,128)(2,1)}), bf16[1,16,4,4096]{3,2,0,1:T(4,128)(2,1)S(1)}, u32[]{:S(2)}, u32[]{:S(2)}) async-start(bf16[1,16,4,4096]{3,2,0,1:T(4,128)(2,1)} %reshape.232), calls=%async_computation.3 | async-start | bytes 1048576 | tf_op jit(solution)/shard_map/all_to_all | solution.py:160
  475.6 0.2 select_reduce_fusion.1
  475.7 0.1 copy.28
  475.8 0.1 reshape.236
  475.9 0.1 copy.24
  476.0 0.1 copy.27
  476.1 54.6 %reduce-scatter.3.cloned.1.call-done = f32[16,4096]{1,0:T(8,128)} async-done(((f32[256,4096]{1,0:T(8,128)}), f32[16,4096]{1,0:T(8,128)}) %reduce-scatter.3.cloned.1.call-update) | async-done | bytes 262160 | tf_op jit(solution)/shard_map/reduce_scatter | solution.py:103
  530.7 1.6 convert_element_type.84
  532.4 0.1 reshape.233
  532.5 0.7 gather_fusion
  533.2 0.2 reshape.235
  533.4 1.5 multiply_reduce_fusion
  (41 shorter events, 0.2 us)
Async XLA Ops:
  7.2 347.7 %copy-start = (bf16[1,128,4096]{2,1,0:T(8,128)(2,1)S(1)}, bf16[1,128,4096]{2,1,0:T(8,128)(2,1)}, u32[]{:S(2)}) copy-start(bf16[1,128,4096]{2,1,0:T(8,128)(2,1)} %param.29) | copy-start | bytes 3145732
  7.2 458.8 %reduce-scatter.5.cloned.1.call-start = ((), (), s32[]{:S(2)}) async-start(), calls=%async_computation.5 | async-start | bytes 17825792 | tf_op jit(solution)/shard_map/reduce_scatter | solution.py:151
  29.7 2.0 collective-permute-start.1
  32.8 25.6 %collective-permute-start.2 = (bf16[2,1,1,64,4096]{4,3,0,2,1:T(8,128)(2,1)}, bf16[2,1,1,64,4096]{4,3,0,2,1:T(8,128)(2,1)S(1)}, u32[]{:S(2)}, u32[]{:S(2)}) collective-permute-start(bf16[2,1,1,64,4096]{4,3,0,2,1:T(8,128)(2,1)} %pad_maximum_fusion.2), channel_id=1, source_target_pairs={{0,2},{1,3},{2,0},{3,1},{4,6},{5,7},{6,4},{7,5},{8,10},{9,11},{10,... | collective-permute-start | bytes 3145736 | tf_op jit(solution)/shard_map/ppermute | solution.py:26
  58.5 1.0 copy-start.5
  58.6 1.3 copy-start.6
  59.9 93.6 %collective-permute-start.3 = (bf16[4,1,1,64,4096]{4,3,0,2,1:T(8,128)(2,1)S(1)}, bf16[4,1,1,64,4096]{4,3,0,2,1:T(8,128)(2,1)}, u32[]{:S(2)}, u32[]{:S(2)}) collective-permute-start(bf16[4,1,1,64,4096]{4,3,0,2,1:T(8,128)(2,1)S(1)} %pad_maximum_fusion.1), channel_id=1, source_target_pairs={{0,4},{1,5},{2,6},{3,7},{4,0},{5,1},{6,2},{7,3},{8,12},{9,13},{10,... | collective-permute-start | bytes 6291464 | tf_op jit(solution)/shard_map/ppermute | solution.py:26
  155.9 2.6 copy-start.2
  158.5 187.5 %collective-permute-start.4 = (bf16[8,1,1,64,4096]{4,3,0,2,1:T(8,128)(2,1)}, bf16[8,1,1,64,4096]{4,3,0,2,1:T(8,128)(2,1)}, u32[]{:S(2)}, u32[]{:S(2)}) collective-permute-start(bf16[8,1,1,64,4096]{4,3,0,2,1:T(8,128)(2,1)} %pad_maximum_fusion), channel_id=1, source_target_pairs={{0,8},{1,9},{2,10},{3,11},{4,12},{5,13},{6,14},{7,15},{8,0},{9,1},... | collective-permute-start | bytes 12582920 | tf_op jit(solution)/shard_map/ppermute | solution.py:26
  164.7 187.6 %copy-start.13 = (bf16[1,4096,128]{2,1,0:T(8,128)(2,1)S(1)}, bf16[1,4096,128]{2,1,0:T(8,128)(2,1)}, u32[]{:S(2)}) copy-start(bf16[1,4096,128]{2,1,0:T(8,128)(2,1)} %param.27) | copy-start | bytes 3145732
  349.1 2.0 copy-start.3
  349.1 3.2 copy-start.4
  352.3 2.6 copy-start.9
  369.3 1.6 copy-start.7
  369.3 2.1 copy-start.10
  369.3 161.4 %reduce-scatter.3.cloned.1.call-start = ((), (), s32[]{:S(2)}) async-start(), calls=%async_computation.4 | async-start | bytes 4456448 | tf_op jit(solution)/shard_map/reduce_scatter | solution.py:103
  370.9 2.7 copy-start.14
  371.4 5.4 copy-start.12
  371.4 8.5 %copy-start.8 = (bf16[128,4096]{1,0:T(8,128)(2,1)S(1)}, bf16[128,4096]{1,0:T(8,128)(2,1)}, u32[]{:S(2)}) copy-start(bf16[128,4096]{1,0:T(8,128)(2,1)} %param.21) | copy-start | bytes 3145732
  374.4 5.5 %collective-permute-start = (bf16[2,128]{1,0:T(2,128)(2,1)S(1)}, bf16[2,128]{1,0:T(2,128)(2,1)S(1)}, u32[]{:S(2)}, u32[]{:S(2)}) collective-permute-start(bf16[2,128]{1,0:T(2,128)(2,1)S(1)} %slice.34), channel_id=1, source_target_pairs={{0,16},{16,32},{32,48},{48,64},{64,80},{80,96},{96,112},{112,128},... | collective-permute-start | bytes 1544 | tf_op jit(solution)/shard_map/ppermute | solution.py:36
  384.5 0.7 copy-start.11
  384.6 0.8 copy-start.16
  384.6 1.9 copy-start.15
  386.5 148.4 %copy-start.1 = (bf16[1,128,4096]{2,1,0:T(8,128)(2,1)S(1)}, bf16[1,128,4096]{2,1,0:T(8,128)(2,1)}, u32[]{:S(2)}) copy-start(bf16[1,128,4096]{2,1,0:T(8,128)(2,1)} %param.29) | copy-start | bytes 3145732
  468.3 64.1 %all-to-all-start.1 = ((bf16[1,16,4,4096]{3,2,0,1:T(4,128)(2,1)}), bf16[1,16,4,4096]{3,2,0,1:T(4,128)(2,1)S(1)}, u32[]{:S(2)}, u32[]{:S(2)}) async-start(bf16[1,16,4,4096]{3,2,0,1:T(4,128)(2,1)} %reshape.232), calls=%async_computation.3 | async-start | bytes 1048576 | tf_op jit(solution)/shard_map/all_to_all | solution.py:160
Sparse Core Ops, SparseCore 0:
  369.4 96.5 reduce-scatter.4
  468.6 62.1 reduce-scatter.2
